TPU v7x, 256 devices: a whole 4x4x8 slice. The times are simulated.
256 devices in a mesh: sp: 128 (over z, y, x), tp: 2 (over core).
Axes of the slice: x: 4, y: 4, z: 8, core: 2. Of those that a mesh axis runs over, the one named last changes fastest.
Arguments:
- queries: bfloat16 [196608, 1024], P('sp', 'tp'), may hold values from -6 to 6
- forget_logit: bfloat16 [196608, 1024], P('sp', 'tp'), may hold values from -8 to 8
- value_rows: bfloat16 [196608, 1024], P('sp', 'tp'), may hold values from -10 to 10
- out_gate: bfloat16 [196608, 1024], P('sp', 'tp'), may hold values from -6 to 6
- floor_gap: float32 [1024], P('tp'), may hold values from 0 to 0.1, as said below
- head_gain: float32 [1024], P('tp'), may hold values from 0.1 to 1.9
- state_in: float32 [8, 128, 128], P('tp'), may hold values from -0.625 to 0.625
- out_weight: bfloat16 [1024, 2048], P('tp'), may hold values from -0.1875 to 0.1875
Outputs:
- projected: bfloat16 [196608, 2048], P(('sp', 'tp'))
- state_out: float32 [8, 16384], P('tp', 'sp')
Inputs may be any that keep to these rules, and one draw needn't show every extreme that they name: `floor_gap`: strictly between 0 and 0.1.
All inputs are finite; a program needn't handle non-finite values.
Results may differ from a plain program's by a relative error of at most 0.009.
Values may be sent and summed in bfloat16 or wider, within the bound.
No kernel may reach another device: no remote copies, remote signals or barrier semaphores. Data moves between devices by JAX's collectives and lax.ppermute only.
A program may use at most 128 MiB of HBM per device.

v0:
```python
import jax
import jax.numpy as jnp
from jax import lax
from jax.sharding import Mesh
from jax.sharding import PartitionSpec as P

BLOCK = 128
SP = ("sp_0", "sp_1", "sp_2")
SP_TP = ("sp_0", "sp_1", "sp_2", "tp")
epsilon = 1e-06


def neutral_like(value, identity):
    return jax.tree.map(
        lambda a, e: jnp.broadcast_to(jnp.asarray(e, a.dtype), a.shape), value, identity
    )


def entering(value, axes, combine, identity):
    before = start = neutral_like(value, identity)
    so_far = value
    for axis in reversed(axes):
        length, mine = (lax.axis_size(axis), lax.axis_index(axis))
        pieces = jax.tree.map(lambda part: lax.all_gather(part, axis), so_far)
        inside, so_far = (start, start)
        for k in range(length):
            passed = k < mine
            so_far = combine(so_far, jax.tree.map(lambda part: part[k], pieces))
            inside = jax.tree.map(lambda new, old: jnp.where(passed, new, old), so_far, inside)
        before = combine(inside, before)
    return before


def broadcast_by_axis(value, axes, root):
    value = jnp.where(lax.axis_index(axes) == root, value, jnp.zeros_like(value))
    for axis in axes:
        value = lax.psum(value, axis)
    return value


def to_blocks(values, head_count):
    blocks = values.shape[0] // BLOCK
    return values.reshape(blocks, BLOCK, head_count, values.shape[1] // head_count)


def join_state(earlier, later):
    return (earlier[0] * later[0], later[0][..., None] * earlier[1] + later[1])


def per_device(
    queries, forget_logit, value_rows, out_gate, floor_gap, head_gain, state_in, out_weight
):
    span_rows = queries.shape[0]
    head_count = state_in.shape[0]
    key_gate = to_blocks(floor_gap * jax.nn.sigmoid(-forget_logit.astype(jnp.float32)), head_count)
    log_forget = jnp.log1p(-key_gate)
    reader = to_blocks(jax.nn.silu(queries.astype(jnp.float32)), head_count)
    written_update = to_blocks(value_rows.astype(jnp.float32), head_count)
    positions = jnp.arange(BLOCK)
    causal = positions[:, None] >= positions[None, :]
    lower_ones = causal.astype(jnp.float32)
    cumul = jnp.einsum("cs,nshk->nchk", lower_ones, log_forget)
    scaled_readout = reader * jnp.exp(cumul)
    key_scaled = key_gate * jnp.exp(-cumul)
    scores = jnp.einsum("nchk,nshk->nhcs", scaled_readout, key_scaled)
    scores = jnp.where(causal, scores, 0.0)
    within = jnp.einsum("nhcs,nshv->nchv", scores, written_update)
    block_log_decay = cumul[:, -1]
    decay_to_finish = key_gate * jnp.exp(block_log_decay[:, None] - cumul)
    segment_state = jnp.einsum("nshk,nshv->nhkv", decay_to_finish, written_update)
    block_final_rows = jnp.cumsum(block_log_decay, axis=0)
    starts = block_final_rows - block_log_decay
    overall_log_decay = block_final_rows[-1]
    block_ids = jnp.arange(block_final_rows.shape[0])
    earlier_mask = (block_ids[:, None] > block_ids[None, :])[:, :, None, None]
    spacing = jnp.where(earlier_mask, starts[:, None] - block_final_rows[None, :], 0.0)
    carry_weight = jnp.where(earlier_mask, jnp.exp(spacing), 0.0)
    local_before = jnp.einsum("jihk,ihkv->jhkv", carry_weight, segment_state)
    decay_dev = jnp.exp(overall_log_decay)
    state_dev = jnp.einsum(
        "lpt,lptr->ptr", jnp.exp(overall_log_decay[None] - block_final_rows), segment_state
    )
    prefix_decay, prefix_state = entering(
        (decay_dev, state_dev),
        SP,
        join_state,
        (jnp.ones_like(decay_dev), jnp.zeros_like(state_dev)),
    )
    incoming = prefix_decay[..., None] * state_in + prefix_state
    before = local_before + jnp.exp(starts)[..., None] * incoming[None]
    unscaled_output = within + jnp.einsum("nchk,nhkv->nchv", scaled_readout, before)
    mean_square = jnp.mean(unscaled_output * unscaled_output, axis=-1, keepdims=True)
    gain_rows = head_gain.reshape(head_count, -1)
    normed = unscaled_output * lax.rsqrt(mean_square + epsilon) * gain_rows
    gating = jax.nn.silu(to_blocks(out_gate.astype(jnp.float32), head_count))
    gated = (normed * gating).astype(jnp.bfloat16).reshape(span_rows, -1)
    regrouped = lax.all_to_all(gated, "tp", split_axis=0, concat_axis=1, tiled=True)
    summed = jnp.dot(
        regrouped,
        lax.all_gather(out_weight, "tp", axis=0, tiled=True),
        preferred_element_type=jnp.float32,
    )
    projected = summed.astype(jnp.bfloat16)
    finished = (decay_dev[..., None] * incoming + state_dev).reshape(head_count, -1)
    whole_final = broadcast_by_axis(
        finished.astype(jnp.bfloat16), SP, lax.axis_size(SP) - 1
    ).astype(finished.dtype)
    share = whole_final.shape[1] // lax.axis_size(SP)
    offset = lax.axis_index(SP) * share
    state_out = lax.dynamic_slice_in_dim(whole_final, offset, share, 1)
    return (projected, state_out)


def solution(mesh):
    torus = Mesh(mesh.devices.reshape(8, 4, 4, mesh.shape["tp"]), ("sp_0", "sp_1", "sp_2", "tp"))
    placed = (
        P(SP, "tp"),
        P(SP, "tp"),
        P(SP, "tp"),
        P(SP, "tp"),
        P("tp"),
        P("tp"),
        P("tp", None, None),
        P("tp", None),
    )
    return jax.shard_map(
        per_device,
        mesh=torus,
        in_specs=placed,
        out_specs=(P(SP_TP, None), P("tp", SP)),
        check_vma=False,
    )
```

profile of v0, /device:TPU:8, one launch (start us, length us, event | category | flops | bytes accessed | tf_op | source)
XLA Modules:
  0.0 314.2 jit_solution(17621082454385104322)
XLA Ops:
  8.0 3.9 %divide_multiply_fusion = f32[1536,512]{1,0:T(8,128)} fusion(bf16[1536,512]{1,0:T(8,128)(2,1)} %param.9, f32[512]{0:T(512)} %param.12), kind=kLoop, calls=%fused_computation.34 | loop fusion | flops 3145728 | bytes 4720640 | tf_op jit(solution)/shard_map/mul | solution.py:55
  11.9 3.1 %reshape.230 = f32[12,128,4,128]{3,2,1,0:T(4,128)S(1)} reshape(f32[1536,512]{1,0:T(8,128)} %divide_multiply_fusion) | data formatting | bytes 6291456 | tf_op jit(solution)/shard_map/reshape | solution.py:43
  15.1 1.7 copy-done
  16.8 2.3 negate_log-plus-one_fusion
  19.9 3.5 %reshape.231 = bf16[12,128,4,128]{3,2,1,0:T(4,128)(2,1)} reshape(bf16[1536,512]{1,0:T(8,128)(2,1)} %param.10) | data formatting | bytes 3145728 | tf_op jit(solution)/shard_map/reshape | solution.py:43
  23.4 3.3 %fusion.15 = bf16[12,4,128,128]{3,2,1,0:T(8,128)(2,1)S(1)} fusion(f32[12,128,4,128]{3,1,2,0:T(8,128)S(1)} %fusion.31, f32[12,128,4,128]{3,2,1,0:T(4,128)} %copy-done, f32[12,4,128]{2,1,0:T(4,128)S(1)} %bitcast.247, bf16[12,128,4,128]{3,2,1,0:T(4,128)(2,1)} %reshape.231), kind=kOutput, calls=%fused_computation.23 | convolution fusion | flops 202899456 | bytes 9461760 | tf_op jit(solution)/shard_map/nshk,nshv->nhkv/dot_general | solution.py:70
  26.7 1.1 copy-done.2
  27.8 1.9 fusion
  29.8 11.2 %all_gather.29 = f32[4,4,128]{2,1,0:T(4,128)S(1)} all-gather(f32[1,4,128]{2,1,0:T(4,128)S(1)} %get-tuple-element.7), channel_id=1, replica_groups=mesh['sp_0'=8,'sp_1'=4,'sp_2'=4,'tp'=2] {'sp_2'}, dimensions={0}, use_global_device_ids=true | all-gather | bytes 10240 | tf_op jit(solution)/shard_map/all_gather | solution.py:24
  41.0 18.4 %all-gather.12.cloned.1.call-done = f32[16,128,128]{2,1,0:T(8,128)} async-done(((f32[4,128,128]{2,1,0:T(8,128)}), f32[16,128,128]{2,1,0:T(8,128)}) %all-gather.12.cloned.1.call-update) | async-done | bytes 1048592 | tf_op jit(solution)/shard_map/all_gather | solution.py:24
  59.4 2.2 bitcast_add_fusion.6
  61.7 10.9 %all_gather.30 = f32[4,4,128]{2,1,0:T(4,128)S(1)} all-gather(f32[1,4,128]{2,1,0:T(4,128)S(1)} %get-tuple-element.20), channel_id=1, replica_groups=mesh['sp_0'=8,'sp_1'=4,'sp_2'=4,'tp'=2] {'sp_1'}, dimensions={0}, use_global_device_ids=true | all-gather | bytes 10240 | tf_op jit(solution)/shard_map/all_gather | solution.py:24
  72.6 15.1 %all-gather.6.cloned.1.call-done = f32[4,4,128,128]{3,2,1,0:T(8,128)} async-done(((f32[1,4,128,128]{3,2,1,0:T(8,128)}), f32[4,4,128,128]{3,2,1,0:T(8,128)}) %all-gather.6.cloned.1.call-update) | async-done | bytes 1048592 | tf_op jit(solution)/shard_map/all_gather | solution.py:24
  87.7 2.2 multiply_add_fusion
  90.1 24.2 %all_gather.31 = f32[8,4,128]{2,1,0:T(4,128)S(1)} all-gather(f32[1,4,128]{2,1,0:T(4,128)S(1)} %get-tuple-element.16), channel_id=1, replica_groups=mesh['sp_0'=8,'sp_1'=4,'sp_2'=4,'tp'=2] {'sp_0'}, dimensions={0}, use_global_device_ids=true | all-gather | bytes 18432 | tf_op jit(solution)/shard_map/all_gather | solution.py:24
  114.3 18.2 %all-gather.8.cloned.1.call-done = f32[8,4,128,128]{3,2,1,0:T(8,128)} async-done(((f32[1,4,128,128]{3,2,1,0:T(8,128)}), f32[8,4,128,128]{3,2,1,0:T(8,128)}) %all-gather.8.cloned.1.call-update) | async-done | bytes 2097168 | tf_op jit(solution)/shard_map/all_gather | solution.py:24
  132.5 4.6 %fusion.68 = (bf16[1,4,128,128]{3,2,1,0:T(8,128)(2,1)S(1)}, f32[4,128,128]{2,1,0:T(8,128)}) fusion(f32[4,128,128]{2,1,0:T(8,128)S(1)} %bitcast.242, f32[4,128]{1,0:T(4,128)S(1)} %fusion.80, pred[]{:T(512)S(6)} %eq.3, pred[]{:T(512)S(6)} %gt.89, pred[]{:T(512)S(6)} %gt.88, pred[]{:T(512)S(6)} %gt.87, f32[16,128,128]{2,1,0:T(8,128)} %all-gather.12.cloned.1.call-done, ...), kind=kLoop, calls=%fused_computation.84 | loop fusion | flops 3604480 | bytes 5152785
  138.0 71.2 %all-reduce.4.cloned.1.call-done = bf16[4,16384]{1,0:T(4,128)(2,1)} async-done(((bf16[4,16384]{1,0:T(4,128)(2,1)}), bf16[4,16384]{1,0:T(4,128)(2,1)}) %all-reduce.4.cloned.1.call-update) | async-done | bytes 131088 | tf_op jit(solution)/shard_map/psum | solution.py:37
  211.1 0.8 copy.33
  211.9 3.9 %convert_multiply_fusion = f32[1536,512]{1,0:T(8,128)} fusion(bf16[1536,512]{1,0:T(8,128)(2,1)} %param.8), kind=kLoop, calls=%fused_computation.9 | loop fusion | flops 3932160 | bytes 4718592 | tf_op jit(solution)/shard_map/jit(silu)/mul | solution.py:57
  215.8 4.9 %reshape.229 = f32[12,128,4,128]{3,2,1,0:T(4,128)} reshape(f32[1536,512]{1,0:T(8,128)} %convert_multiply_fusion) | data formatting | bytes 6291456 | tf_op jit(solution)/shard_map/reshape | solution.py:43
  220.7 4.3 %reshape.235 = f32[12,128,4,128]{3,2,1,0:T(4,128)} reshape(bf16[1536,512]{1,0:T(8,128)(2,1)} %param.11) | data formatting | bytes 4718592 | tf_op jit(solution)/shard_map/reshape | solution.py:43
  225.0 4.7 %copy.39 = f32[12,128,4,128]{1,3,2,0:T(8,128)} copy(f32[12,128,4,128]{3,2,1,0:T(4,128)} %reshape.235) | data formatting | bytes 6291456 | tf_op jit(solution)/shard_map/reshape | solution.py:43
  229.7 4.4 %bitcast_add_fusion = bf16[12,4,128,128]{3,0,2,1:T(8,128)(2,1)S(1)} fusion(f32[4,128,128]{2,1,0:T(8,128)} %get-tuple-element.3, f32[12,4,128]{0,2,1:T(8,128)} %copy.36, f32[12,4,128]{0,2,1:T(8,128)S(1)} %copy.34, f32[12,4,128]{0,2,1:T(8,128)} %copy.33, pred[12,12]{1,0:T(8,128)(4,1)S(1)} %iota_compare_fusion.2, bf16[12,4,128,128]{3,2,1,0:T(8,128)(2,1)} %copy-done.2), kind=kOutput, calls=%fused_computation.4 | convolution fusion | flops 21454848 | bytes 3481744 | tf_op jit(solution)/shard_map/jihk,ihkv->jhkv/dot_general | solution.py:78
  234.2 2.9 fusion.11
  237.1 8.2 %multiply_reduce_fusion = (f32[12,128,4]{1,2,0:T(4,128)S(1)}, f32[12,128,4,128]{1,3,2,0:T(8,128)}) fusion(f32[12,4,128,128]{3,2,1,0:T(8,128)} %fusion.11, bf16[12,128,4,128]{3,2,1,0:T(4,128)(2,1)} %reshape.231, pred[128,128]{1,0:T(8,128)(4,1)S(1)} %iota_compare_fusion, f32[12,128,4,128]{3,1,2,0:T(8,128)S(1)} %fusion.31, f32[12,128,4,128]{3,2,1,0:T(4,128)} %copy-done, ...), kind=kOutput, calls=%fused_computation.22 | convolution fusion | flops 408152064 | bytes 17342464 | tf_op jit(solution)/shard_map/nhcs,nshv->nchv/dot_general | solution.py:67
  245.3 3.9 %multiply_convert_fusion = bf16[12,128,4,128]{1,3,2,0:T(8,128)(2,1)S(1)} fusion(f32[12,128,4,128]{1,3,2,0:T(8,128)} %copy.39, f32[12,128,4,128]{1,3,2,0:T(8,128)} %get-tuple-element.25, f32[4,128]{1,0:T(4,128)S(1)} %bitcast.251, f32[12,128,4]{1,2,0:T(4,128)S(1)} %add_rsqrt_fusion), kind=kLoop, calls=%fused_computation.21 | loop fusion | flops 6291456 | bytes 7890944 | tf_op jit(solution)/shard_map/convert_element_type | solution.py:96
  249.2 1.1 copy.40
  250.9 5.0 %all_to_all.19 = bf16[2,768,512]{2,1,0:T(8,128)(2,1)S(1)} all-to-all(bf16[2,768,512]{2,1,0:T(8,128)(2,1)S(1)} %all_to_all.14), channel_id=1, replica_groups=mesh['sp_0'=8,'sp_1'=4,'sp_2'=4,'tp'=2] {'tp'}, dimensions={0} | all-to-all | bytes 3145728 | tf_op jit(solution)/shard_map/all_to_all | solution.py:97
  256.7 7.0 %convolution_convert_fusion = bf16[768,2048]{1,0:T(8,128)(2,1)} fusion(bf16[768,1024]{0,1:T(8,128)(2,1)S(1)} %bitcast.240, bf16[1024,2048]{1,0:T(8,128)(2,1)} %all-gather.10.cloned.1.call-done), kind=kOutput, calls=%fused_computation.11 | convolution fusion | flops 3222798336 | bytes 8912896 | tf_op jit(solution)/shard_map/dot_general | solution.py:98
  263.7 41.8 %all-reduce.8.cloned.1.call-done = bf16[4,16384]{1,0:T(4,128)(2,1)} async-done(((bf16[4,16384]{1,0:T(4,128)(2,1)}), bf16[4,16384]{1,0:T(4,128)(2,1)}) %all-reduce.8.cloned.1.call-update) | async-done | bytes 131088 | tf_op jit(solution)/shard_map/psum | solution.py:37
  305.5 1.2 dynamic-slice_convert_fusion
  (48 shorter events, 5.2 us)
Async XLA Ops:
  8.0 51.4 %all-gather.12.cloned.1.call-start = ((), (), s32[]{:S(2)}) async-start(), calls=%async_computation.7 | async-start | bytes 1310720 | tf_op jit(solution)/shard_map/all_gather | solution.py:24
  15.1 1.7 copy-start
  26.7 1.1 copy-start.2
  29.7 102.8 %copy-start.3 = (f32[4,128,1,128]{3,2,1,0:T(1,128)S(1)}, f32[4,128,1,128]{3,2,1,0:T(1,128)}, u32[]{:S(2)}) copy-start(f32[4,128,1,128]{3,2,1,0:T(1,128)} %fusion) | copy-start | bytes 786436
  29.8 58.0 %all-gather.6.cloned.1.call-start = ((), (), s32[]{:S(2)}) async-start(), calls=%async_computation.1 | async-start | bytes 1310720 | tf_op jit(solution)/shard_map/all_gather | solution.py:24
  61.7 70.8 %all-gather.8.cloned.1.call-start = ((), (), s32[]{:S(2)}) async-start(), calls=%async_computation.2 | async-start | bytes 2359296 | tf_op jit(solution)/shard_map/all_gather | solution.py:24
  90.0 119.2 %all-reduce.4.cloned.1.call-start = ((), (), s32[]{:S(2)}) async-start(), calls=%async_computation.4 | async-start | bytes 262144 | tf_op jit(solution)/shard_map/psum | solution.py:37
  137.9 118.7 %all-reduce.6.cloned.1.call-start = ((), (), s32[]{:S(2)}) async-start(), calls=%async_computation.5 | async-start | bytes 262144 | tf_op jit(solution)/shard_map/psum | solution.py:37
  209.2 47.5 %all-gather.10.cloned.1.call-start = ((), (), s32[]{:S(2)}) async-start(), calls=%async_computation.3 | async-start | bytes 6291456 | tf_op jit(solution)/shard_map/all_gather | solution.py:100
  209.8 95.8 %all-reduce.8.cloned.1.call-start = ((), (), s32[]{:S(2)}) async-start(), calls=%async_computation.6 | async-start | bytes 262144 | tf_op jit(solution)/shard_map/psum | solution.py:37
  229.7 4.4 %copy-start.1 = (f32[12,128,4,128]{3,2,1,0:T(4,128)S(1)}, f32[12,128,4,128]{3,2,1,0:T(4,128)}, u32[]{:S(2)}) copy-start(f32[12,128,4,128]{3,2,1,0:T(4,128)} %reshape.229) | copy-start | bytes 9437188
  237.1 8.2 %copy-start.4 = (f32[512]{0:T(512)S(1)}, f32[512]{0:T(512)}, u32[]{:S(2)}) copy-start(f32[512]{0:T(512)} %param.13) | copy-start | bytes 6148
Sparse Core Ops, SparseCore 0:
  29.9 29.4 all-gather.11
  61.8 25.8 all-gather.5
  90.1 42.3 all-gather.7
  138.0 71.0 all-reduce.3
  211.3 43.8 all-reduce.5
  257.4 48.0 all-reduce.7
Sparse Core Ops, SparseCore 1:
  211.5 17.4 all-gather.9
where the time goes:
time: 315 us; the launch traced here: 314 us
  waiting for transfers between devices  165 us (52%)
  blocking collectives  51.2 us (16%)
  local copies, waits for them, and re-layouts  28.6 us (9%)
  matrix products  28.3 us (9%)
  other arithmetic  24.4 us (8%)
  between operations  15.8 us (5%)
    psum x3, waiting for transfers between devices, broadcast_by_axis(): value = lax.psum(value, axis)  113 us
    all_gather x3, waiting for transfers between devices, entering(): pieces = jax.tree.map(lambda part: lax.all_gather(part, axis), so_far)  51.7 us
    all_gather x3, blocking collectives, entering(): pieces = jax.tree.map(lambda part: lax.all_gather(part, axis), so_far)  46.2 us
    reshape x5, local copies, waits for them, and re-layouts, to_blocks(): values.reshape(blocks, BLOCK, head_count, values.shape[1] // head_count)  20.5 us
    dot_general x1, matrix products, per_device(): within = jnp.einsum('nhcs,nshv->nchv', scores, written_update)  8.21 us
    dot_general x1, matrix products, per_device(): jnp.dot(regrouped, lax.all_gather(out_weight, 'tp', axis=0, tiled=True),...  7.04 us
  transfers between devices with their start and end apart: 7, of which 5 were waited for; matrix products, arithmetic and copies ran while one was open for 15% of the time, Pallas kernels for 0%

commit v1 on v0

--- a/solution.py
+++ b/solution.py
@@ -34,7 +34,7 @@
 def broadcast_by_axis(value, axes, root):
     value = jnp.where(lax.axis_index(axes) == root, value, jnp.zeros_like(value))
     for axis in axes:
-        value = lax.psum(value, axis)
+        value = jnp.sum(lax.all_gather(value, axis), axis=0)
     return value
 
 

time: 315 us -> 230 us (0.73)
  waiting for transfers between devices: 165 us -> 49.1 us
  blocking collectives: 51.2 us -> 77.2 us
  other arithmetic: 24.4 us -> 28.1 us
    psum x3 -> x0, waiting for transfers between devices: 113 us -> none  [broadcast_by_axis(): value = lax.psum(value, axis)]
    all_gather x0 -> x2, blocking collectives: none -> 25.9 us  [broadcast_by_axis(): value = jnp.sum(lax.all_gather(value, axis), axis=0)]
    all_gather x3, waiting for transfers between devices: 51.7 us -> 33.5 us  [entering(): pieces = jax.tree.map(lambda part: lax.all_gather(part, axis), so_far)]
    all_gather x0 -> x1, waiting for transfers between devices: none -> 15 us  [broadcast_by_axis(): value = jnp.sum(lax.all_gather(value, axis), axis=0)]
    select_n x0 -> x1, other arithmetic: none -> 4.82 us  [broadcast_by_axis(): jnp.where(lax.axis_index(axes) == root, value, jnp.zeros_like(value))]
    unnamed x1 -> x0, other arithmetic: 4.63 us -> none
  transfers between devices with their start and end apart: 7 -> 5, of which waited for: 5 -> 3; matrix products, arithmetic and copies ran while one was open for 15% -> 25% of each run, Pallas kernels for 0% -> 0%
where the time goes in v1:
time: 230 us; the launch traced here: 229 us
  blocking collectives  77.2 us (34%)
  waiting for transfers between devices  49.1 us (21%)
  local copies, waits for them, and re-layouts  31.3 us (14%)
  matrix products  28.5 us (12%)
  other arithmetic  28.1 us (12%)
  between operations  14.1 us (6%)
    all_gather x3, blocking collectives, entering(): pieces = jax.tree.map(lambda part: lax.all_gather(part, axis), so_far)  46.3 us
    all_gather x3, waiting for transfers between devices, entering(): pieces = jax.tree.map(lambda part: lax.all_gather(part, axis), so_far)  33.5 us
    all_gather x2, blocking collectives, broadcast_by_axis(): value = jnp.sum(lax.all_gather(value, axis), axis=0)  25.9 us
    reshape x5, local copies, waits for them, and re-layouts, to_blocks(): values.reshape(blocks, BLOCK, head_count, values.shape[1] // head_count)  20.6 us
    all_gather x1, waiting for transfers between devices, broadcast_by_axis(): value = jnp.sum(lax.all_gather(value, axis), axis=0)  15 us
    dot_general x1, matrix products, per_device(): within = jnp.einsum('nhcs,nshv->nchv', scores, written_update)  8.21 us
    dot_general x1, matrix products, per_device(): jnp.dot(regrouped, lax.all_gather(out_weight, 'tp', axis=0, tiled=True),...  7.07 us
    all_to_all x1, blocking collectives, per_device(): lax.all_to_all(gated, 'tp', split_axis=0, concat_axis=1, tiled=True)  5 us
  transfers between devices with their start and end apart: 5, of which 3 were waited for; matrix products, arithmetic and copies ran while one was open for 25% of the time, Pallas kernels for 0%

profile of v1, /device:TPU:8, one launch (start us, length us, event | category | flops | bytes accessed | tf_op | source)
XLA Modules:
  0.0 228.5 jit_solution(11606101350447418665)
XLA Ops:
  7.2 3.9 %divide_multiply_fusion = f32[1536,512]{1,0:T(8,128)} fusion(bf16[1536,512]{1,0:T(8,128)(2,1)} %param.9, f32[512]{0:T(512)} %param.12), kind=kLoop, calls=%fused_computation.34 | loop fusion | flops 3145728 | bytes 4720640 | tf_op jit(solution)/shard_map/mul | solution.py:55
  11.1 3.1 %reshape.243 = f32[12,128,4,128]{3,2,1,0:T(4,128)S(1)} reshape(f32[1536,512]{1,0:T(8,128)} %divide_multiply_fusion) | data formatting | bytes 6291456 | tf_op jit(solution)/shard_map/reshape | solution.py:43
  14.3 1.7 copy-done
  16.0 2.3 negate_log-plus-one_fusion
  18.9 0.9 copy.44
  19.8 3.5 %reshape.244 = bf16[12,128,4,128]{3,2,1,0:T(4,128)(2,1)} reshape(bf16[1536,512]{1,0:T(8,128)(2,1)} %param.10) | data formatting | bytes 3145728 | tf_op jit(solution)/shard_map/reshape | solution.py:43
  23.3 3.3 %fusion.15 = bf16[12,4,128,128]{3,2,1,0:T(8,128)(2,1)S(1)} fusion(f32[12,128,4,128]{3,1,2,0:T(8,128)S(1)} %fusion.31, f32[12,128,4,128]{3,2,1,0:T(4,128)} %copy-done, f32[12,4,128]{2,1,0:T(4,128)S(1)} %bitcast.245, bf16[12,128,4,128]{3,2,1,0:T(4,128)(2,1)} %reshape.244), kind=kOutput, calls=%fused_computation.23 | convolution fusion | flops 202899456 | bytes 9461760 | tf_op jit(solution)/shard_map/nshk,nshv->nhkv/dot_general | solution.py:70
  26.6 1.2 copy-done.2
  27.8 1.9 fusion
  29.7 11.2 %all_gather.45 = f32[4,4,128]{2,1,0:T(4,128)S(1)} all-gather(f32[1,4,128]{2,1,0:T(4,128)S(1)} %get-tuple-element.7), channel_id=1, replica_groups=mesh['sp_0'=8,'sp_1'=4,'sp_2'=4,'tp'=2] {'sp_2'}, dimensions={0}, use_global_device_ids=true | all-gather | bytes 10240 | tf_op jit(solution)/shard_map/all_gather | solution.py:24
  40.9 18.4 %all-gather.19.cloned.1.call-done = f32[16,128,128]{2,1,0:T(8,128)} async-done(((f32[4,128,128]{2,1,0:T(8,128)}), f32[16,128,128]{2,1,0:T(8,128)}) %all-gather.19.cloned.1.call-update) | async-done | bytes 1048592 | tf_op jit(solution)/shard_map/all_gather | solution.py:24
  59.3 2.2 bitcast_add_fusion.6
  61.6 10.9 %all_gather.46 = f32[4,4,128]{2,1,0:T(4,128)S(1)} all-gather(f32[1,4,128]{2,1,0:T(4,128)S(1)} %get-tuple-element.20), channel_id=1, replica_groups=mesh['sp_0'=8,'sp_1'=4,'sp_2'=4,'tp'=2] {'sp_1'}, dimensions={0}, use_global_device_ids=true | all-gather | bytes 10240 | tf_op jit(solution)/shard_map/all_gather | solution.py:24
  72.6 15.1 %all-gather.11.cloned.1.call-done = f32[4,4,128,128]{3,2,1,0:T(8,128)} async-done(((f32[1,4,128,128]{3,2,1,0:T(8,128)}), f32[4,4,128,128]{3,2,1,0:T(8,128)}) %all-gather.11.cloned.1.call-update) | async-done | bytes 1048592 | tf_op jit(solution)/shard_map/all_gather | solution.py:24
  87.6 2.2 multiply_add_fusion
  93.2 3.9 %convert_multiply_fusion = f32[1536,512]{1,0:T(8,128)} fusion(bf16[1536,512]{1,0:T(8,128)(2,1)} %param.8), kind=kLoop, calls=%fused_computation.9 | loop fusion | flops 3932160 | bytes 4718592 | tf_op jit(solution)/shard_map/jit(silu)/mul | solution.py:57
  97.1 4.9 %reshape.242 = f32[12,128,4,128]{3,2,1,0:T(4,128)} reshape(f32[1536,512]{1,0:T(8,128)} %convert_multiply_fusion) | data formatting | bytes 6291456 | tf_op jit(solution)/shard_map/reshape | solution.py:43
  102.1 4.1 %reshape.248 = f32[12,128,4,128]{3,2,1,0:T(4,128)} reshape(bf16[1536,512]{1,0:T(8,128)(2,1)} %param.11) | data formatting | bytes 4718592 | tf_op jit(solution)/shard_map/reshape | solution.py:43
  106.2 4.9 %copy.39 = f32[12,128,4,128]{1,3,2,0:T(8,128)} copy(f32[12,128,4,128]{3,2,1,0:T(4,128)} %reshape.248) | data formatting | bytes 6291456 | tf_op jit(solution)/shard_map/reshape | solution.py:43
  111.1 24.3 %all_gather.47 = f32[8,4,128]{2,1,0:T(4,128)S(1)} all-gather(f32[1,4,128]{2,1,0:T(4,128)S(1)} %get-tuple-element.16), channel_id=1, replica_groups=mesh['sp_0'=8,'sp_1'=4,'sp_2'=4,'tp'=2] {'sp_0'}, dimensions={0}, use_global_device_ids=true | all-gather | bytes 18432 | tf_op jit(solution)/shard_map/all_gather | solution.py:24
  138.4 4.8 %fusion.67 = (bf16[4,128,128]{2,1,0:T(8,128)(2,1)S(1)}, f32[4,128,128]{2,1,0:T(8,128)}) fusion(f32[4,128,128]{2,1,0:T(8,128)S(1)} %bitcast.239, f32[4,128]{1,0:T(4,128)} %fusion.79, pred[]{:T(512)S(6)} %eq.3, pred[]{:T(512)S(6)} %gt.89, pred[]{:T(512)S(6)} %gt.88, pred[]{:T(512)S(6)} %gt.87, f32[16,128,128]{2,1,0:T(8,128)} %all-gather.19.cloned.1.call-done, ...), kind=kLoop, calls=%fused_computation.83 | loop fusion | flops 3604480 | bytes 5152785 | tf_op jit(solution)/shard_map/jit(_where)/select_n | solution.py:35
  143.9 4.6 %bitcast_add_fusion = bf16[12,4,128,128]{3,0,2,1:T(8,128)(2,1)S(1)} fusion(f32[4,128,128]{2,1,0:T(8,128)} %get-tuple-element.3, f32[12,4,128]{0,2,1:T(8,128)} %copy.36, f32[12,4,128]{0,2,1:T(8,128)} %copy.34, f32[12,4,128]{0,2,1:T(8,128)} %copy.33, pred[12,12]{1,0:T(8,128)(4,1)} %iota_compare_fusion.2, bf16[12,4,128,128]{3,2,1,0:T(8,128)(2,1)} %copy-done.2), kind=kOutput, calls=%fused_computation.4 | convolution fusion | flops 21454848 | bytes 3481744 | tf_op jit(solution)/shard_map/jihk,ihkv->jhkv/dot_general | solution.py:78
  148.5 2.9 %fusion.11 = f32[12,4,128,128]{3,2,1,0:T(8,128)} fusion(bf16[12,4,128,128]{3,0,2,1:T(8,128)(2,1)S(1)} %bitcast_add_fusion, f32[12,128,4,128]{3,2,1,0:T(4,128)S(1)} %copy-done.1, f32[12,128,4,128]{3,1,2,0:T(8,128)S(1)} %fusion.31), kind=kOutput, calls=%fused_computation.16 | convolution fusion | flops 202113024 | bytes 11010048 | tf_op jit(solution)/shard_map/nchk,nhkv->nchv/dot_general | solution.py:91
  151.5 8.2 %multiply_reduce_fusion = (f32[12,128,4]{1,2,0:T(4,128)S(1)}, f32[12,128,4,128]{1,3,2,0:T(8,128)}) fusion(f32[12,4,128,128]{3,2,1,0:T(8,128)} %fusion.11, bf16[12,128,4,128]{3,2,1,0:T(4,128)(2,1)} %reshape.244, pred[128,128]{1,0:T(8,128)(4,1)S(1)} %iota_compare_fusion, f32[12,128,4,128]{3,1,2,0:T(8,128)S(1)} %fusion.31, f32[12,128,4,128]{3,2,1,0:T(4,128)} %copy-done, ...), kind=kOutput, calls=%fused_computation.22 | convolution fusion | flops 408152064 | bytes 17342464 | tf_op jit(solution)/shard_map/nhcs,nshv->nchv/dot_general | solution.py:67
  159.7 3.9 %multiply_convert_fusion = bf16[12,128,4,128]{1,3,2,0:T(8,128)(2,1)S(1)} fusion(f32[12,128,4,128]{1,3,2,0:T(8,128)} %copy.39, f32[12,128,4,128]{1,3,2,0:T(8,128)} %get-tuple-element.25, f32[4,128]{1,0:T(4,128)S(1)} %bitcast.249, f32[12,128,4]{1,2,0:T(4,128)S(1)} %add_rsqrt_fusion), kind=kLoop, calls=%fused_computation.21 | loop fusion | flops 6291456 | bytes 7890944 | tf_op jit(solution)/shard_map/convert_element_type | solution.py:96
  163.6 1.1 copy.40
  165.3 5.0 %all_to_all.19 = bf16[2,768,512]{2,1,0:T(8,128)(2,1)S(1)} all-to-all(bf16[2,768,512]{2,1,0:T(8,128)(2,1)S(1)} %all_to_all.14), channel_id=1, replica_groups=mesh['sp_0'=8,'sp_1'=4,'sp_2'=4,'tp'=2] {'tp'}, dimensions={0} | all-to-all | bytes 3145728 | tf_op jit(solution)/shard_map/all_to_all | solution.py:97
  171.1 7.1 %convolution_convert_fusion = bf16[768,2048]{1,0:T(8,128)(2,1)} fusion(bf16[768,1024]{0,1:T(8,128)(2,1)S(1)} %bitcast.237, bf16[1024,2048]{1,0:T(8,128)(2,1)} %all-gather.15.cloned.1.call-done), kind=kOutput, calls=%fused_computation.11 | convolution fusion | flops 3222798336 | bytes 8912896 | tf_op jit(solution)/shard_map/dot_general | solution.py:98
  178.1 15.0 %all-gather.17.cloned.1.call-done = bf16[8,4,16384]{2,1,0:T(4,128)(2,1)} async-done(((bf16[1,4,16384]{2,1,0:T(4,128)(2,1)}), bf16[8,4,16384]{2,1,0:T(4,128)(2,1)}) %all-gather.17.cloned.1.call-update) | async-done | bytes 1048592 | tf_op jit(solution)/shard_map/all_gather | solution.py:37
  193.1 1.7 reduce_sum.46
  194.9 12.8 %all-gather.3 = bf16[4,4,16384]{2,1,0:T(4,128)(2,1)S(1)} all-gather(bf16[1,4,16384]{2,1,0:T(4,128)(2,1)S(1)} %bitcast.242), channel_id=3, replica_groups=mesh['sp_0'=8,'sp_1'=4,'sp_2'=4,'tp'=2] {'sp_1'}, dimensions={0}, use_global_device_ids=true | all-gather | bytes 655360 | tf_op jit(solution)/shard_map/all_gather | solution.py:37
  208.0 13.1 %all-gather.4 = bf16[4,4,16384]{2,1,0:T(4,128)(2,1)S(1)} all-gather(bf16[1,4,16384]{2,1,0:T(4,128)(2,1)S(1)} %bitcast.243), channel_id=4, replica_groups=mesh['sp_0'=8,'sp_1'=4,'sp_2'=4,'tp'=2] {'sp_2'}, dimensions={0}, use_global_device_ids=true | all-gather | bytes 655360 | tf_op jit(solution)/shard_map/all_gather | solution.py:37
  (65 shorter events, 10.4 us)
Async XLA Ops:
  7.2 52.2 %all-gather.19.cloned.1.call-start = ((), (), s32[]{:S(2)}) async-start(), calls=%async_computation.5 | async-start | bytes 1310720 | tf_op jit(solution)/shard_map/all_gather | solution.py:24
  14.3 1.7 copy-start
  23.3 4.5 %copy-start.4 = (bf16[12,4,128,1]{0,3,2,1:T(2,128)(2,1)S(1)}, bf16[12,4,128,1]{0,3,2,1:T(2,128)(2,1)}, u32[]{:S(2)}) copy-start(bf16[12,4,128,1]{0,3,2,1:T(2,128)(2,1)} %copy.44) | copy-start | bytes 36868
  26.6 1.2 copy-start.2
  29.7 58.0 %all-gather.11.cloned.1.call-start = ((), (), s32[]{:S(2)}) async-start(), calls=%async_computation.1 | async-start | bytes 1310720 | tf_op jit(solution)/shard_map/all_gather | solution.py:24
  40.9 31.6 %copy-start.7 = (f32[4,128]{1,0:T(4,128)}, f32[4,128]{1,0:T(4,128)S(1)}, u32[]{:S(2)}) copy-start(f32[4,128]{1,0:T(4,128)S(1)} %get-tuple-element.21) | copy-start | bytes 6148
  40.9 50.5 %copy-start.8 = (f32[4,128]{1,0:T(4,128)}, f32[4,128]{1,0:T(4,128)S(1)}, u32[]{:S(2)}) copy-start(f32[4,128]{1,0:T(4,128)S(1)} %get-tuple-element.22) | copy-start | bytes 6148
  40.9 50.5 %copy-start.9 = (f32[4,128]{1,0:T(4,128)}, f32[4,128]{1,0:T(4,128)S(1)}, u32[]{:S(2)}) copy-start(f32[4,128]{1,0:T(4,128)S(1)} %get-tuple-element.23) | copy-start | bytes 6148
  40.9 50.5 %copy-start.5 = (f32[4,128]{1,0:T(4,128)}, f32[4,128]{1,0:T(4,128)S(1)}, u32[]{:S(2)}) copy-start(f32[4,128]{1,0:T(4,128)S(1)} %bitcast_multiply_fusion) | copy-start | bytes 6148
  61.6 76.8 %all-gather.13.cloned.1.call-start = ((), (), s32[]{:S(2)}) async-start(), calls=%async_computation.2 | async-start | bytes 2359296 | tf_op jit(solution)/shard_map/all_gather | solution.py:24
  72.5 18.9 %copy-start.10 = (f32[4,128]{1,0:T(4,128)}, f32[4,128]{1,0:T(4,128)S(1)}, u32[]{:S(2)}) copy-start(f32[4,128]{1,0:T(4,128)S(1)} %get-tuple-element.17) | copy-start | bytes 6148
  72.5 18.9 %copy-start.11 = (f32[4,128]{1,0:T(4,128)}, f32[4,128]{1,0:T(4,128)S(1)}, u32[]{:S(2)}) copy-start(f32[4,128]{1,0:T(4,128)S(1)} %get-tuple-element.18) | copy-start | bytes 6148
  72.5 24.6 %copy-start.12 = (f32[4,128]{1,0:T(4,128)}, f32[4,128]{1,0:T(4,128)S(1)}, u32[]{:S(2)}) copy-start(f32[4,128]{1,0:T(4,128)S(1)} %get-tuple-element.19) | copy-start | bytes 6148
  72.6 18.9 %copy-start.6 = (f32[4,128]{1,0:T(4,128)}, f32[4,128]{1,0:T(4,128)S(1)}, u32[]{:S(2)}) copy-start(f32[4,128]{1,0:T(4,128)S(1)} %bitcast_multiply_fusion.2) | copy-start | bytes 6148
  89.9 81.2 %all-gather.15.cloned.1.call-start = ((), (), s32[]{:S(2)}) async-start(), calls=%async_computation.3 | async-start | bytes 6291456 | tf_op jit(solution)/shard_map/all_gather | solution.py:100
  90.5 102.6 %all-gather.17.cloned.1.call-start = ((), (), s32[]{:S(2)}) async-start(), calls=%async_computation.4 | async-start | bytes 1179648 | tf_op jit(solution)/shard_map/all_gather | solution.py:37
  106.2 32.3 %copy-start.3 = (f32[4,128,1,128]{3,2,1,0:T(1,128)S(1)}, f32[4,128,1,128]{3,2,1,0:T(1,128)}, u32[]{:S(2)}) copy-start(f32[4,128,1,128]{3,2,1,0:T(1,128)} %fusion) | copy-start | bytes 786436
  143.9 4.6 %copy-start.1 = (f32[12,128,4,128]{3,2,1,0:T(4,128)S(1)}, f32[12,128,4,128]{3,2,1,0:T(4,128)}, u32[]{:S(2)}) copy-start(f32[12,128,4,128]{3,2,1,0:T(4,128)} %reshape.242) | copy-start | bytes 9437188
  151.5 8.2 %copy-start.13 = (f32[512]{0:T(512)S(1)}, f32[512]{0:T(512)}, u32[]{:S(2)}) copy-start(f32[512]{0:T(512)} %param.13) | copy-start | bytes 6148
Sparse Core Ops, SparseCore 0:
  29.8 29.4 all-gather.18
  61.7 25.8 all-gather.10
  90.0 42.4 all-gather.12
  134.2 17.5 all-gather.14
  153.4 39.7 all-gather.16
